TPU v7x, 32 devices: a whole 2x2x4 slice. The times are simulated.
32 devices in a mesh: kv: 16 (over z, y, x), tp: 2 (over core).
Axes of the slice: x: 2, y: 2, z: 4, core: 2. Of those that a mesh axis runs over, the one named last changes fastest.
Arguments:
- hidden_in: bfloat16 [64, 2048], P('tp', 'kv'), may hold values from -20 to 20
- gain_before: float32 [2048], P('kv'), may hold values from 0.1 to 1.9
- gate_before: bfloat16 [2048, 5632], P('kv', 'tp'), may hold values from -0.125 to 0.125
- lift_before: bfloat16 [2048, 5632], P('kv', 'tp'), may hold values from -0.125 to 0.125
- drop_before: bfloat16 [5632, 2048], P('tp', 'kv'), may hold values from -0.078125 to 0.078125
- mixer_gain: float32 [2048], P('kv'), may hold values from 0.1 to 1.9
- value_proj: bfloat16 [2048, 2048], P('kv', 'tp'), may hold values from -0.125 to 0.125
- gate_proj: bfloat16 [2048, 2048], P('kv', 'tp'), may hold values from -0.125 to 0.125
- key_proj: bfloat16 [2048, 1024], P('kv', 'tp'), may hold values from -0.125 to 0.125
- query_proj: bfloat16 [2048, 1024], P('kv', 'tp'), may hold values from -0.125 to 0.125
- step_proj: bfloat16 [2048, 32], P('kv'), may hold values from -0.125 to 0.125
- value_taps: float32 [4, 2048], P(None, 'tp'), may hold values from -3 to 3
- key_taps: float32 [4, 1024], P(None, 'tp'), may hold values from -3 to 3
- query_taps: float32 [4, 1024], P(None, 'tp'), may hold values from -3 to 3
- value_past: bfloat16 [64, 3, 2048], P('kv', None, 'tp'), may hold values from -6 to 6
- key_past: bfloat16 [64, 3, 1024], P('kv', None, 'tp'), may hold values from -6 to 6
- query_past: bfloat16 [64, 3, 1024], P('kv', None, 'tp'), may hold values from -6 to 6
- decay_rate: float32 [32], P('tp'), may hold values from 0.05 to 1
- block_state: float32 [64, 32, 64, 128], P('kv', 'tp'), may hold values from -24 to 24
- block_keys: bfloat16 [64, 128, 1024], P('kv', None, 'tp'), may hold values from -6 to 6
- block_values: bfloat16 [64, 128, 2048], P('kv', None, 'tp'), may hold values from -6 to 6
- block_steps: float32 [64, 128, 32], P('kv', None, 'tp'), may hold values from 0.2 to 2
- block_decay: float32 [64, 128, 32], P('kv', None, 'tp'), may hold values from -1.25 to 0
- lengths: int32 [64], P('kv'), may hold values from 1 to 128, 2048 in all
- head_gain: float32 [2048], P('tp'), may hold values from 0.1 to 1.9
- out_proj: bfloat16 [2048, 2048], P('tp', 'kv'), may hold values from -0.125 to 0.125
- gain_after: float32 [2048], P('kv'), may hold values from 0.1 to 1.9
- gate_after: bfloat16 [2048, 5632], P('kv', 'tp'), may hold values from -0.125 to 0.125
- lift_after: bfloat16 [2048, 5632], P('kv', 'tp'), may hold values from -0.125 to 0.125
- drop_after: bfloat16 [5632, 2048], P('tp', 'kv'), may hold values from -0.078125 to 0.078125
Outputs:
- hidden_out: bfloat16 [64, 2048], P('tp', 'kv')
Inputs may be any that keep to these rules, and one draw needn't show every extreme that they name: `lengths`: some sequence has all 128 positions filled.
All inputs are finite; a program needn't handle non-finite values. No bound on the sum of `lengths` on one device may be relied on, other than what follows from the above.
Results may differ from a plain program's by a relative error of at most 0.014.
Values may be sent and summed in bfloat16 or wider, within the bound.
A program may use at most 64 MiB of HBM per device.

v0:
```python
import jax
import jax.numpy as jnp
from jax import lax
from jax.sharding import PartitionSpec as P

D = 2048
GROUPS = 8
HEADS = 32
EPSILON = 1e-06


def gather_rows(rows_in, gain_vec):
    whole_rows = lax.all_gather(rows_in, "tp", axis=0, tiled=True)
    values = whole_rows.astype(jnp.float32)
    squares = jnp.sum(values * values, axis=1)
    scaled = (values * gain_vec[None, :]).astype(jnp.bfloat16)
    return (scaled, squares)


def inverse_scale(totals):
    return lax.rsqrt(totals / D + EPSILON)[:, None]


def own_rows(totals, row_count):
    return lax.dynamic_slice_in_dim(totals, lax.axis_index("kv") * row_count, row_count, 0)


def finish(partial_value):
    return lax.psum_scatter(
        partial_value.astype(jnp.float32).astype(jnp.bfloat16),
        "tp",
        scatter_dimension=0,
        tiled=True,
    ).astype(jnp.float32)


def half_mlp(rows_in, gain_vec, gate_weight, lift_weight, drop_weight):
    scaled, squares = gather_rows(rows_in, gain_vec)
    totals = lax.psum(squares, "kv")
    gate_part = jnp.dot(scaled, gate_weight, preferred_element_type=jnp.float32)
    lift_part = jnp.dot(scaled, lift_weight, preferred_element_type=jnp.float32)
    gate_sum, lift_sum = lax.psum((gate_part, lift_part), "kv")
    row_scale = inverse_scale(totals)
    hidden = (jax.nn.silu(gate_sum * row_scale) * (lift_sum * row_scale)).astype(jnp.bfloat16)
    partial_value = jnp.dot(hidden, drop_weight, preferred_element_type=jnp.float32).astype(
        jnp.bfloat16
    )
    return finish(partial_value)


def convolve(past_rows, taps, newest):
    earlier = jnp.sum(past_rows.astype(jnp.float32) * taps[None, :-1, :], axis=1)
    return jax.nn.silu(earlier + taps[-1][None, :] * newest)


def mixer(
    rows_in,
    mixer_gain,
    value_proj,
    gate_proj,
    key_proj,
    query_proj,
    step_proj,
    value_taps,
    key_taps,
    query_taps,
    value_past,
    key_past,
    query_past,
    decay_rate,
    block_state,
    block_keys,
    block_values,
    block_steps,
    block_decay,
    lengths,
    head_gain,
    out_proj,
):
    scaled, squares = gather_rows(rows_in, mixer_gain)
    seq_count = lengths.shape[0]
    value_part = jnp.dot(scaled, value_proj, preferred_element_type=jnp.float32)
    gate_part = jnp.dot(scaled, gate_proj, preferred_element_type=jnp.float32)
    key_part = jnp.dot(scaled, key_proj, preferred_element_type=jnp.float32)
    query_part = jnp.dot(scaled, query_proj, preferred_element_type=jnp.float32)
    step_part = jnp.dot(scaled, step_proj, preferred_element_type=jnp.float32)
    totals = own_rows(lax.psum(squares, "kv"), seq_count)
    value_raw, gate_raw, key_raw, query_raw, step_all = (
        lax.psum_scatter(value_part, "kv", scatter_dimension=0, tiled=True),
        lax.psum_scatter(gate_part, "kv", scatter_dimension=0, tiled=True),
        lax.psum_scatter(key_part, "kv", scatter_dimension=0, tiled=True),
        lax.psum_scatter(query_part, "kv", scatter_dimension=0, tiled=True),
        lax.psum_scatter(step_part, "kv", scatter_dimension=0, tiled=True),
    )
    row_scale = inverse_scale(totals)
    heads_here = decay_rate.shape[0]
    step_raw = (
        lax.dynamic_slice_in_dim(step_all, lax.axis_index("tp") * heads_here, heads_here, 1)
        * row_scale
    )
    new_value = convolve(value_past, value_taps, value_raw * row_scale)
    gate_vals = gate_raw * row_scale
    new_key = convolve(key_past, key_taps, key_raw * row_scale)
    new_query = convolve(query_past, query_taps, query_raw * row_scale)
    step_size = jax.nn.softplus(step_raw)
    new_decay = -decay_rate[None, :] * step_size
    block_len = block_keys.shape[1]
    head_dim = block_state.shape[2]
    state_size = block_state.shape[3]
    per_group = HEADS // GROUPS
    group_count = heads_here // per_group
    live_mask = (jnp.arange(block_len, dtype=jnp.int32)[None, :] < (lengths - 1)[:, None])[
        :, :, None
    ]
    masked = jnp.where(live_mask, block_decay, 0.0)
    running = jnp.cumsum(masked, axis=1)
    block_total = running[:, -1, :]
    tail_sum = block_total[:, None, :] - running
    query_round = new_query.astype(jnp.bfloat16).reshape(seq_count, group_count, state_size)
    scores = jnp.einsum(
        "slgn,sgn->slg",
        block_keys.reshape(seq_count, block_len, group_count, state_size),
        query_round,
        preferred_element_type=jnp.float32,
    )
    scores = jnp.repeat(scores, per_group, axis=2)
    weights = jnp.where(
        live_mask, jnp.exp(tail_sum + new_decay[:, None, :]) * block_steps * scores, 0.0
    ).astype(jnp.bfloat16)
    from_block = jnp.einsum(
        "slh,slhp->shp",
        weights,
        block_values.reshape(seq_count, block_len, heads_here, head_dim),
        preferred_element_type=jnp.float32,
    )
    query_heads = jnp.repeat(
        new_query.reshape(seq_count, group_count, state_size), per_group, axis=1
    )
    source_state = jnp.einsum(
        "shpn,shn->shp", block_state, query_heads, precision=lax.Precision.HIGHEST
    )
    source_state = source_state * jnp.exp(block_total + new_decay)[:, :, None]
    self_score = jnp.repeat(
        jnp.sum((new_query * new_key).reshape(seq_count, group_count, state_size), axis=2),
        per_group,
        axis=1,
    )
    from_token = (step_size * self_score)[:, :, None] * new_value.reshape(
        seq_count, heads_here, head_dim
    )
    gated_out = (source_state + from_block + from_token) * jax.nn.silu(
        gate_vals.reshape(seq_count, heads_here, head_dim)
    )
    normed = gated_out * lax.rsqrt(jnp.mean(gated_out * gated_out, axis=2, keepdims=True) + EPSILON)
    normed = normed * head_gain.reshape(heads_here, head_dim)[None]
    mixed_rows = normed.reshape(seq_count, heads_here * head_dim).astype(jnp.bfloat16)
    partial_value = jnp.dot(
        lax.all_gather(mixed_rows, "kv", axis=0, tiled=True),
        out_proj,
        preferred_element_type=jnp.float32,
    ).astype(jnp.bfloat16)
    return finish(partial_value)


def on_device(
    hidden_in,
    gain_before,
    gate_before,
    lift_before,
    drop_before,
    mixer_gain,
    value_proj,
    gate_proj,
    key_proj,
    query_proj,
    step_proj,
    value_taps,
    key_taps,
    query_taps,
    value_past,
    key_past,
    query_past,
    decay_rate,
    block_state,
    block_keys,
    block_values,
    block_steps,
    block_decay,
    lengths,
    head_gain,
    out_proj,
    gain_after,
    gate_after,
    lift_after,
    drop_after,
):
    section_one = (
        hidden_in.astype(jnp.float32)
        + 0.5 * half_mlp(hidden_in, gain_before, gate_before, lift_before, drop_before)
    ).astype(jnp.bfloat16)
    branch_mix = mixer(
        section_one,
        mixer_gain,
        value_proj,
        gate_proj,
        key_proj,
        query_proj,
        step_proj,
        value_taps,
        key_taps,
        query_taps,
        value_past,
        key_past,
        query_past,
        decay_rate,
        block_state,
        block_keys,
        block_values,
        block_steps,
        block_decay,
        lengths,
        head_gain,
        out_proj,
    )
    section_two = (section_one.astype(jnp.float32) + branch_mix).astype(jnp.bfloat16)
    return (
        section_two.astype(jnp.float32)
        + 0.5 * half_mlp(section_two, gain_after, gate_after, lift_after, drop_after)
    ).astype(jnp.bfloat16)


def solution(mesh):
    return jax.shard_map(
        on_device,
        mesh=mesh,
        in_specs=(
            P("tp", "kv"),
            P("kv"),
            P("kv", "tp"),
            P("kv", "tp"),
            P("tp", "kv"),
            P("kv"),
            P("kv", "tp"),
            P("kv", "tp"),
            P("kv", "tp"),
            P("kv", "tp"),
            P("kv", None),
            P(None, "tp"),
            P(None, "tp"),
            P(None, "tp"),
            P("kv", None, "tp"),
            P("kv", None, "tp"),
            P("kv", None, "tp"),
            P("tp"),
            P("kv", "tp", None, None),
            P("kv", None, "tp"),
            P("kv", None, "tp"),
            P("kv", None, "tp"),
            P("kv", None, "tp"),
            P("kv"),
            P("tp"),
            P("tp", "kv"),
            P("kv"),
            P("kv", "tp"),
            P("kv", "tp"),
            P("tp", "kv"),
        ),
        out_specs=P("tp", "kv"),
        check_vma=False,
    )
```

profile of v0, /device:TPU:0, one launch (start us, length us, event | category | flops | bytes accessed | tf_op | source)
XLA Modules:
  0.0 464.0 jit_solution(2448503861973463744)
XLA Ops:
  6.5 2.3 all_gather.12
  8.8 2.2 fusion.13
  11.1 2.2 fusion.15
  13.5 43.7 %psum.50 = f32[64]{0:T(128)S(1)} all-reduce(f32[64]{0:T(128)S(1)} %fusion.2), channel_id=1, replica_groups=mesh['kv'=16,'tp'=2] {'kv'}, use_global_device_ids=true, to_apply=%region_2.0 | all-reduce | flops 64 | bytes 512 | tf_op jit(solution)/shard_map/psum | solution.py:39
  57.2 75.0 %all-reduce.17.cloned.1.call-done = (f32[64,2816]{1,0:T(8,128)}, f32[64,2816]{1,0:T(8,128)}) async-done(((f32[64,2816]{1,0:T(8,128)}, f32[64,2816]{1,0:T(8,128)}), (f32[64,2816]{1,0:T(8,128)}, f32[64,2816]{1,0:T(8,128)})) %all-reduce.17.cloned.1.call-update) | async-done | bytes 1441808 | tf_op jit(solution)/shard_map/psum | solution.py:42
  132.2 2.6 convolution_convert_fusion.1
  135.0 7.0 %reduce-scatter.4.cloned.1.call-done = bf16[32,128]{1,0:T(8,128)(2,1)} async-done(((bf16[64,128]{1,0:T(8,128)(2,1)}), bf16[32,128]{1,0:T(8,128)(2,1)}) %reduce-scatter.4.cloned.1.call-update) | async-done | bytes 8208 | tf_op jit(solution)/shard_map/reduce_scatter | solution.py:29
  142.0 0.7 add_convert_fusion.2
  142.7 1.8 all_gather.13
  144.6 0.9 fusion.22
  145.5 0.9 fusion.24
  146.3 0.8 fusion.26
  147.1 0.8 fusion.30
  148.2 0.3 copy.54
  148.5 0.1 copy.43
  148.6 0.3 reduce_window_sum.11
  148.9 0.6 dynamic-slice
  150.3 2.3 copy.46
  152.8 0.1 fusion.28
  153.0 77.1 %all-reduce.5 = (f32[64]{0:T(128)S(1)}, f32[64,32]{1,0:T(8,128)S(1)}) all-reduce(f32[64]{0:T(128)S(1)} %fusion.4, f32[64,32]{1,0:T(8,128)S(1)} %fusion.28), channel_id=1, replica_groups=mesh['kv'=16,'tp'=2] {'kv'}, use_global_device_ids=true, to_apply=%region_8.9 | all-reduce | flops 2112 | bytes 16896 | tf_op jit(solution)/shard_map/psum | solution.py:87
  230.2 30.9 %all-reduce.15.cloned.1.call-done = (f32[64,1024]{1,0:T(8,128)}, f32[64,1024]{1,0:T(8,128)}, f32[64,512]{1,0:T(8,128)}, f32[64,512]{1,0:T(8,128)}) async-done(((f32[64,1024]{1,0:T(8,128)}, f32[64,1024]{1,0:T(8,128)}, f32[64,512]{1,0:T(8,128)}, f32[64,512]{1,0:T(8,128)}), (f32[64,1024]{1,0:T(8,128)}, f32[64,1024]{1,0:T(8,128)}, f32[64,512]{1,0:T(8,128)}, f32[64,512]{1,0:T(8,128)})) %all-reduce.15.cloned.1.call-update) | async-done | bytes 786448
  261.1 0.8 fusion.17
  262.0 0.2 fusion.36
  262.2 0.1 copy.45
  262.6 0.7 add_exponential_fusion
  263.3 0.1 fusion
  263.6 0.9 divide_multiply_fusion
  264.5 0.7 reshape.84
  265.1 0.7 reshape.85
  265.8 1.9 fusion.37
  267.8 3.4 fusion.35
  271.2 0.9 multiply_reduce_fusion.1
  272.0 0.7 multiply_convert_fusion.4
  272.7 0.8 reshape.86
  273.5 41.6 %all-gather = bf16[16,4,1024]{2,1,0:T(4,128)(2,1)} all-gather(bf16[1,4,1024]{2,1,0:T(4,128)(2,1)S(1)} %reshape.86), channel_id=1, replica_groups=mesh['kv'=16,'tp'=2] {'kv'}, dimensions={0}, use_global_device_ids=true | all-gather | bytes 139264 | tf_op jit(solution)/shard_map/all_gather | solution.py:158
  315.1 1.6 reshape.87
  316.7 1.8 convolution_convert_fusion.2
  318.6 3.5 reduce-scatter.6.cloned.1.call-done
  322.0 0.7 add_convert_fusion.1
  322.7 0.6 copy-done.10
  323.3 1.8 all_gather.15
  325.1 1.8 fusion.11
  326.9 1.8 fusion.9
  328.9 42.2 %psum.54 = f32[64]{0:T(128)S(1)} all-reduce(f32[64]{0:T(128)S(1)} %fusion.6), channel_id=1, replica_groups=mesh['kv'=16,'tp'=2] {'kv'}, use_global_device_ids=true, to_apply=%region_21.22 | all-reduce | flops 64 | bytes 512 | tf_op jit(solution)/shard_map/psum | solution.py:39
  371.1 75.0 %all-reduce.13.cloned.1.call-done = (f32[64,2816]{1,0:T(8,128)}, f32[64,2816]{1,0:T(8,128)}) async-done(((f32[64,2816]{1,0:T(8,128)}, f32[64,2816]{1,0:T(8,128)}), (f32[64,2816]{1,0:T(8,128)}, f32[64,2816]{1,0:T(8,128)})) %all-reduce.13.cloned.1.call-update) | async-done | bytes 1441808 | tf_op jit(solution)/shard_map/psum | solution.py:42
  446.1 2.6 convolution_convert_fusion
  448.7 7.2 %reduce-scatter.8.cloned.1.call-done = bf16[32,128]{1,0:T(8,128)(2,1)} async-done(((bf16[64,128]{1,0:T(8,128)(2,1)}), bf16[32,128]{1,0:T(8,128)(2,1)}) %reduce-scatter.8.cloned.1.call-update) | async-done | bytes 8208 | tf_op jit(solution)/shard_map/reduce_scatter | solution.py:29
  455.8 1.3 add_convert_fusion
  (98 shorter events, 1.7 us)
Async XLA Ops:
  6.5 261.3 %copy-start = (f32[4,16,64,128]{3,2,1,0:T(8,128)S(1)}, f32[4,16,64,128]{3,2,1,0:T(8,128)}, u32[]{:S(2)}) copy-start(f32[4,16,64,128]{3,2,1,0:T(8,128)} %param.48) | copy-start | bytes 6291460
  6.5 125.6 %all-reduce.17.cloned.1.call-start = ((), (), s32[]{:S(2)}) async-start(), calls=%async_computation.8 | async-start | bytes 2883584 | tf_op jit(solution)/shard_map/psum | solution.py:42
  8.8 48.4 %copy-start.26 = (s32[4]{0:T(128)S(1)}, s32[4]{0:T(128)}, u32[]{:S(2)}) copy-start(s32[4]{0:T(128)} %param.53) | copy-start | bytes 52
  13.3 128.7 %reduce-scatter.4.cloned.1.call-start = ((), (), s32[]{:S(2)}) async-start(), calls=%async_computation.3 | async-start | bytes 24576 | tf_op jit(solution)/shard_map/reduce_scatter | solution.py:29
  132.2 9.9 %copy-start.13 = (bf16[32,128]{1,0:T(8,128)(2,1)S(1)}, bf16[32,128]{1,0:T(8,128)(2,1)}, u32[]{:S(2)}) copy-start(bf16[32,128]{1,0:T(8,128)(2,1)} %param.30) | copy-start | bytes 24580
  132.2 12.4 %copy-start.4 = (bf16[128,1024]{1,0:T(8,128)(2,1)S(1)}, bf16[128,1024]{1,0:T(8,128)(2,1)}, u32[]{:S(2)}) copy-start(bf16[128,1024]{1,0:T(8,128)(2,1)} %param.37) | copy-start | bytes 786436
  132.2 12.4 %copy-start.17 = (f32[128]{0:T(128)S(1)}, f32[128]{0:T(128)}, u32[]{:S(2)}) copy-start(f32[128]{0:T(128)} %param.35) | copy-start | bytes 1540
  132.2 13.3 %copy-start.5 = (bf16[128,1024]{1,0:T(8,128)(2,1)S(1)}, bf16[128,1024]{1,0:T(8,128)(2,1)}, u32[]{:S(2)}) copy-start(bf16[128,1024]{1,0:T(8,128)(2,1)} %param.36) | copy-start | bytes 786436
  132.2 14.2 %copy-start.6 = (bf16[128,512]{1,0:T(8,128)(2,1)S(1)}, bf16[128,512]{1,0:T(8,128)(2,1)}, u32[]{:S(2)}) copy-start(bf16[128,512]{1,0:T(8,128)(2,1)} %param.38) | copy-start | bytes 393220
  132.2 14.9 %copy-start.7 = (bf16[128,512]{1,0:T(8,128)(2,1)S(1)}, bf16[128,512]{1,0:T(8,128)(2,1)}, u32[]{:S(2)}) copy-start(bf16[128,512]{1,0:T(8,128)(2,1)} %param.39) | copy-start | bytes 393220
  134.8 13.2 %copy-start.14 = (f32[4,128,16]{1,2,0:T(8,128)S(1)}, f32[4,128,16]{1,2,0:T(8,128)}, u32[]{:S(2)}) copy-start(f32[4,128,16]{1,2,0:T(8,128)} %param.52) | copy-start | bytes 98308
  134.8 13.2 %copy-start.19 = (f32[4,512]{1,0:T(4,128)S(1)}, f32[4,512]{1,0:T(4,128)}, u32[]{:S(2)}) copy-start(f32[4,512]{1,0:T(4,128)} %param.43) | copy-start | bytes 24580
  134.8 13.2 %copy-start.18 = (f32[4,512]{1,0:T(4,128)S(1)}, f32[4,512]{1,0:T(4,128)}, u32[]{:S(2)}) copy-start(f32[4,512]{1,0:T(4,128)} %param.42) | copy-start | bytes 24580
  134.8 13.3 %copy-start.3 = (bf16[4,128,512]{2,1,0:T(8,128)(2,1)S(1)}, bf16[4,128,512]{2,1,0:T(8,128)(2,1)}, u32[]{:S(2)}) copy-start(bf16[4,128,512]{2,1,0:T(8,128)(2,1)} %param.49) | copy-start | bytes 1572868
  134.9 126.2 %all-reduce.15.cloned.1.call-start = ((), (), s32[]{:S(2)}) async-start(), calls=%async_computation.7 | async-start | bytes 1572864
  135.0 13.1 %copy-start.24 = (pred[4,128]{1,0:T(4,128)(4,1)}, pred[4,128]{1,0:T(4,128)(4,1)S(1)}, u32[]{:S(2)}) copy-start(pred[4,128]{1,0:T(4,128)(4,1)S(1)} %iota_compare_fusion) | copy-start | bytes 1540
  144.6 4.3 copy-start.28
  144.6 5.6 %copy-start.27 = (f32[16]{0:T(128)S(1)}, f32[16]{0:T(128)}, u32[]{:S(2)}) copy-start(f32[16]{0:T(128)} %param.47) | copy-start | bytes 196
  144.6 5.6 %copy-start.12 = (f32[4,128,16]{1,2,0:T(8,128)S(1)}, f32[4,128,16]{1,2,0:T(8,128)}, u32[]{:S(2)}) copy-start(f32[4,128,16]{1,2,0:T(8,128)} %param.51) | copy-start | bytes 98308
  148.0 174.1 %reduce-scatter.6.cloned.1.call-start = ((), (), s32[]{:S(2)}) async-start(), calls=%async_computation.4 | async-start | bytes 24576 | tf_op jit(solution)/shard_map/reduce_scatter | solution.py:29
  148.1 4.4 copy-start.15
  148.1 4.4 copy-start.23
  148.1 4.5 copy-start.16
  148.1 4.5 copy-start.20
  148.2 4.5 copy-start.21
  148.2 4.7 %copy-start.22 = (bf16[128,32]{0,1:T(8,128)(2,1)S(1)}, bf16[128,32]{0,1:T(8,128)(2,1)}, u32[]{:S(2)}) copy-start(bf16[128,32]{0,1:T(8,128)(2,1)} %param.40) | copy-start | bytes 24580
  148.6 114.7 %copy-start.25 = (pred[4,128]{1,0:T(4,128)(4,1)S(1)}, pred[4,128]{1,0:T(4,128)(4,1)}, u32[]{:S(2)}) copy-start(pred[4,128]{1,0:T(4,128)(4,1)} %copy-done.24) | copy-start | bytes 1540
  265.8 5.3 %copy-start.8 = (f32[4,16,64]{2,1,0:T(8,128)S(1)}, f32[4,16,64]{2,1,0:T(8,128)}, u32[]{:S(2)}) copy-start(f32[4,16,64]{2,1,0:T(8,128)} %reshape.84) | copy-start | bytes 49156
  265.8 5.3 %copy-start.9 = (f32[4,16,64]{2,1,0:T(8,128)S(1)}, f32[4,16,64]{2,1,0:T(8,128)}, u32[]{:S(2)}) copy-start(f32[4,16,64]{2,1,0:T(8,128)} %reshape.85) | copy-start | bytes 49156
  265.8 59.3 %copy-start.1 = (bf16[128,2816]{1,0:T(8,128)(2,1)S(1)}, bf16[128,2816]{1,0:T(8,128)(2,1)}, u32[]{:S(2)}) copy-start(bf16[128,2816]{1,0:T(8,128)(2,1)} %param.57) | copy-start | bytes 2162692
  267.8 59.1 %copy-start.2 = (bf16[128,2816]{1,0:T(8,128)(2,1)S(1)}, bf16[128,2816]{1,0:T(8,128)(2,1)}, u32[]{:S(2)}) copy-start(bf16[128,2816]{1,0:T(8,128)(2,1)} %param.58) | copy-start | bytes 2162692
  318.5 127.6 %all-reduce.13.cloned.1.call-start = ((), (), s32[]{:S(2)}) async-start(), calls=%async_computation.6 | async-start | bytes 2883584 | tf_op jit(solution)/shard_map/psum | solution.py:42
  322.7 0.6 copy-start.10
  328.7 127.1 %reduce-scatter.8.cloned.1.call-start = ((), (), s32[]{:S(2)}) async-start(), calls=%async_computation.5 | async-start | bytes 24576 | tf_op jit(solution)/shard_map/reduce_scatter | solution.py:29
  446.1 9.8 %copy-start.11 = (bf16[32,128]{1,0:T(8,128)(2,1)S(1)}, bf16[32,128]{1,0:T(8,128)(2,1)}, u32[]{:S(2)}) copy-start(bf16[32,128]{1,0:T(8,128)(2,1)} %copy-done.10) | copy-start | bytes 24580
Sparse Core Ops, SparseCore 0:
  13.5 118.6 all-reduce.16
  135.0 6.9 reduce-scatter.3
  148.1 112.9 all-reduce.14
  318.6 3.3 reduce-scatter.5
  328.8 117.2 all-reduce.12
  448.8 6.9 reduce-scatter.7
where the time goes:
time: 465 us; the launch traced here: 464 us
  blocking collectives  211 us (45%)
  waiting for transfers between devices  199 us (43%)
  matrix products  24 us (5%)
  between operations  14.5 us (3%)
  local copies, waits for them, and re-layouts  8.42 us (2%)
  other arithmetic  7.7 us (2%)
    psum x2, waiting for transfers between devices, half_mlp(): gate_sum, lift_sum = lax.psum((gate_part, lift_part), 'kv')  150 us
    psum x2, blocking collectives, half_mlp(): totals = lax.psum(squares, 'kv')  85.9 us
    psum x1, blocking collectives, mixer(): totals = own_rows(lax.psum(squares, 'kv'), seq_count)  77.1 us
    all_gather x1, blocking collectives, mixer(): lax.all_gather(mixed_rows, 'kv', axis=0, tiled=True)  41.6 us
    unnamed x7, waiting for transfers between devices  31 us
    reduce_scatter x3, waiting for transfers between devices, finish(): lax.psum_scatter(partial_value.astype(jnp.float32).astype(jnp.bfloat16),...  17.7 us
  transfers between devices with their start and end apart: 6, of which 6 were waited for; matrix products, arithmetic and copies ran while one was open for 1% of the time, Pallas kernels for 0%

commit v1 on v0

--- a/solution.py
+++ b/solution.py
@@ -36,7 +36,10 @@
 
 def half_mlp(rows_in, gain_vec, gate_weight, lift_weight, drop_weight):
     scaled, squares = gather_rows(rows_in, gain_vec)
-    totals = lax.psum(squares, "kv")
+    size, totals = (lax.axis_size("kv"), squares)
+    for reach in [1 << k for k in range(size.bit_length() - 1)]:
+        swap = [(i, i ^ reach) for i in range(size)]
+        totals = totals + lax.ppermute(totals, "kv", swap)
     gate_part = jnp.dot(scaled, gate_weight, preferred_element_type=jnp.float32)
     lift_part = jnp.dot(scaled, lift_weight, preferred_element_type=jnp.float32)
     gate_sum, lift_sum = lax.psum((gate_part, lift_part), "kv")

time: 465 us -> 465 us (level)
  blocking collectives: 211 us -> 125 us
  waiting for transfers between devices: 199 us -> 267 us
  starting transfers between devices: 0.21 us -> 17.6 us
    psum x2 -> x0, blocking collectives: 85.9 us -> none  [half_mlp(): totals = lax.psum(squares, 'kv')]
    psum x2, waiting for transfers between devices: 150 us -> 204 us  [half_mlp(): gate_sum, lift_sum = lax.psum((gate_part, lift_part), 'kv')]
    ppermute x0 -> x8, starting transfers between devices: none -> 17.4 us  [half_mlp(): totals = totals + lax.ppermute(totals, 'kv', swap)]
    ppermute x0 -> x8, waiting for transfers between devices: none -> 14.7 us  [half_mlp(): totals = totals + lax.ppermute(totals, 'kv', swap)]
  transfers between devices with their start and end apart: 6 -> 14, of which waited for: 6 -> 14; matrix products, arithmetic and copies ran while one was open for 1% -> 1% of each run, Pallas kernels for 0% -> 0%
where the time goes in v1:
time: 465 us; the launch traced here: 464 us
  waiting for transfers between devices  267 us (57%)
  blocking collectives  125 us (27%)
  matrix products  24 us (5%)
  starting transfers between devices  17.6 us (4%)
  between operations  14.5 us (3%)
  local copies, waits for them, and re-layouts  8.43 us (2%)
  other arithmetic  7.72 us (2%)
    psum x2, waiting for transfers between devices, half_mlp(): gate_sum, lift_sum = lax.psum((gate_part, lift_part), 'kv')  204 us
    psum x1, blocking collectives, mixer(): totals = own_rows(lax.psum(squares, 'kv'), seq_count)  77.2 us
    all_gather x1, blocking collectives, mixer(): lax.all_gather(mixed_rows, 'kv', axis=0, tiled=True)  41.6 us
    unnamed x7, waiting for transfers between devices  31 us
    reduce_scatter x3, waiting for transfers between devices, finish(): lax.psum_scatter(partial_value.astype(jnp.float32).astype(jnp.bfloat16),...  17.7 us
    ppermute x8, starting transfers between devices, half_mlp(): totals = totals + lax.ppermute(totals, 'kv', swap)  17.4 us
    ppermute x8, waiting for transfers between devices, half_mlp(): totals = totals + lax.ppermute(totals, 'kv', swap)  14.7 us
  transfers between devices with their start and end apart: 14, of which 14 were waited for; matrix products, arithmetic and copies ran while one was open for 1% of the time, Pallas kernels for 0%

profile of v1, /device:TPU:0, one launch (start us, length us, event | category | flops | bytes accessed | tf_op | source)
XLA Modules:
  0.0 464.1 jit_solution(13339581685637497307)
XLA Ops:
  6.5 2.3 all_gather.12
  8.8 2.3 fusion.13
  11.1 2.2 fusion.15
  13.5 2.9 collective-permute-start
  16.4 1.5 collective-permute-done
  18.0 2.0 collective-permute-start.1
  20.0 1.5 collective-permute-done.1
  21.6 2.1 collective-permute-start.2
  23.6 2.0 collective-permute-done.2
  25.6 2.7 collective-permute-start.3
  28.4 1.8 collective-permute-done.3
  30.1 102.0 %all-reduce.17.cloned.1.call-done = (f32[64,2816]{1,0:T(8,128)}, f32[64,2816]{1,0:T(8,128)}) async-done(((f32[64,2816]{1,0:T(8,128)}, f32[64,2816]{1,0:T(8,128)}), (f32[64,2816]{1,0:T(8,128)}, f32[64,2816]{1,0:T(8,128)})) %all-reduce.17.cloned.1.call-update) | async-done | bytes 1441808 | tf_op jit(solution)/shard_map/psum | solution.py:45
  132.2 2.6 convolution_convert_fusion.1
  135.0 7.0 %reduce-scatter.4.cloned.1.call-done = bf16[32,128]{1,0:T(8,128)(2,1)} async-done(((bf16[64,128]{1,0:T(8,128)(2,1)}), bf16[32,128]{1,0:T(8,128)(2,1)}) %reduce-scatter.4.cloned.1.call-update) | async-done | bytes 8208 | tf_op jit(solution)/shard_map/reduce_scatter | solution.py:29
  142.0 0.7 add_convert_fusion.2
  142.7 1.8 all_gather.13
  144.6 0.9 fusion.22
  145.4 0.9 fusion.24
  146.3 0.8 fusion.26
  147.2 0.8 fusion.30
  150.3 2.3 copy.46
  153.0 77.2 %all-reduce.5 = (f32[64]{0:T(128)S(1)}, f32[64,32]{1,0:T(8,128)S(1)}) all-reduce(f32[64]{0:T(128)S(1)} %fusion.4, f32[64,32]{1,0:T(8,128)S(1)} %fusion.28), channel_id=1, replica_groups=mesh['kv'=16,'tp'=2] {'kv'}, use_global_device_ids=true, to_apply=%region_7.8 | all-reduce | flops 2112 | bytes 16896 | tf_op jit(solution)/shard_map/psum | solution.py:90
  230.2 30.9 %all-reduce.15.cloned.1.call-done = (f32[64,1024]{1,0:T(8,128)}, f32[64,1024]{1,0:T(8,128)}, f32[64,512]{1,0:T(8,128)}, f32[64,512]{1,0:T(8,128)}) async-done(((f32[64,1024]{1,0:T(8,128)}, f32[64,1024]{1,0:T(8,128)}, f32[64,512]{1,0:T(8,128)}, f32[64,512]{1,0:T(8,128)}), (f32[64,1024]{1,0:T(8,128)}, f32[64,1024]{1,0:T(8,128)}, f32[64,512]{1,0:T(8,128)}, f32[64,512]{1,0:T(8,128)})) %all-reduce.15.cloned.1.call-update) | async-done | bytes 786448
  261.1 0.8 fusion.17
  263.6 0.9 divide_multiply_fusion
  265.9 1.9 fusion.37
  267.9 3.4 fusion.35
  271.2 0.9 multiply_reduce_fusion.1
  272.8 0.8 reshape.86
  273.6 41.6 %all-gather = bf16[16,4,1024]{2,1,0:T(4,128)(2,1)} all-gather(bf16[1,4,1024]{2,1,0:T(4,128)(2,1)S(1)} %reshape.86), channel_id=1, replica_groups=mesh['kv'=16,'tp'=2] {'kv'}, dimensions={0}, use_global_device_ids=true | all-gather | bytes 139264 | tf_op jit(solution)/shard_map/all_gather | solution.py:161
  315.2 1.6 reshape.87
  316.7 1.8 convolution_convert_fusion.2
  318.6 3.5 reduce-scatter.6.cloned.1.call-done
  323.4 1.8 all_gather.15
  325.2 1.8 fusion.11
  327.0 1.8 fusion.9
  328.9 1.8 collective-permute-start.4
  330.7 1.9 collective-permute-done.4
  332.6 1.7 collective-permute-start.5
  334.3 1.9 collective-permute-done.5
  336.1 1.7 collective-permute-start.6
  337.8 2.1 collective-permute-done.6
  340.0 2.5 collective-permute-start.7
  342.5 2.0 collective-permute-done.7
  344.5 101.7 %all-reduce.13.cloned.1.call-done = (f32[64,2816]{1,0:T(8,128)}, f32[64,2816]{1,0:T(8,128)}) async-done(((f32[64,2816]{1,0:T(8,128)}, f32[64,2816]{1,0:T(8,128)}), (f32[64,2816]{1,0:T(8,128)}, f32[64,2816]{1,0:T(8,128)})) %all-reduce.13.cloned.1.call-update) | async-done | bytes 1441808 | tf_op jit(solution)/shard_map/psum | solution.py:45
  446.2 2.6 convolution_convert_fusion
  448.7 7.2 %reduce-scatter.8.cloned.1.call-done = bf16[32,128]{1,0:T(8,128)(2,1)} async-done(((bf16[64,128]{1,0:T(8,128)(2,1)}), bf16[32,128]{1,0:T(8,128)(2,1)}) %reduce-scatter.8.cloned.1.call-update) | async-done | bytes 8208 | tf_op jit(solution)/shard_map/reduce_scatter | solution.py:29
  455.9 1.3 add_convert_fusion
  (118 shorter events, 7.6 us)
Async XLA Ops:
  6.5 261.3 %copy-start = (f32[4,16,64,128]{3,2,1,0:T(8,128)S(1)}, f32[4,16,64,128]{3,2,1,0:T(8,128)}, u32[]{:S(2)}) copy-start(f32[4,16,64,128]{3,2,1,0:T(8,128)} %param.48) | copy-start | bytes 6291460
  6.5 125.6 %all-reduce.17.cloned.1.call-start = ((), (), s32[]{:S(2)}) async-start(), calls=%async_computation.8 | async-start | bytes 2883584 | tf_op jit(solution)/shard_map/psum | solution.py:45
  8.8 19.5 %copy-start.26 = (s32[4]{0:T(128)S(1)}, s32[4]{0:T(128)}, u32[]{:S(2)}) copy-start(s32[4]{0:T(128)} %param.53) | copy-start | bytes 52
  13.4 128.6 %reduce-scatter.4.cloned.1.call-start = ((), (), s32[]{:S(2)}) async-start(), calls=%async_computation.3 | async-start | bytes 24576 | tf_op jit(solution)/shard_map/reduce_scatter | solution.py:29
  13.5 4.4 collective-permute-start
  18.0 3.6 collective-permute-start.1
  21.6 4.1 collective-permute-start.2
  25.6 4.5 collective-permute-start.3
  132.1 9.8 %copy-start.13 = (bf16[32,128]{1,0:T(8,128)(2,1)S(1)}, bf16[32,128]{1,0:T(8,128)(2,1)}, u32[]{:S(2)}) copy-start(bf16[32,128]{1,0:T(8,128)(2,1)} %param.30) | copy-start | bytes 24580
  132.2 12.4 %copy-start.4 = (bf16[128,1024]{1,0:T(8,128)(2,1)S(1)}, bf16[128,1024]{1,0:T(8,128)(2,1)}, u32[]{:S(2)}) copy-start(bf16[128,1024]{1,0:T(8,128)(2,1)} %param.37) | copy-start | bytes 786436
  132.2 12.4 %copy-start.17 = (f32[128]{0:T(128)S(1)}, f32[128]{0:T(128)}, u32[]{:S(2)}) copy-start(f32[128]{0:T(128)} %param.35) | copy-start | bytes 1540
  132.2 13.3 %copy-start.5 = (bf16[128,1024]{1,0:T(8,128)(2,1)S(1)}, bf16[128,1024]{1,0:T(8,128)(2,1)}, u32[]{:S(2)}) copy-start(bf16[128,1024]{1,0:T(8,128)(2,1)} %param.36) | copy-start | bytes 786436
  132.2 14.2 %copy-start.6 = (bf16[128,512]{1,0:T(8,128)(2,1)S(1)}, bf16[128,512]{1,0:T(8,128)(2,1)}, u32[]{:S(2)}) copy-start(bf16[128,512]{1,0:T(8,128)(2,1)} %param.38) | copy-start | bytes 393220
  132.2 15.0 %copy-start.7 = (bf16[128,512]{1,0:T(8,128)(2,1)S(1)}, bf16[128,512]{1,0:T(8,128)(2,1)}, u32[]{:S(2)}) copy-start(bf16[128,512]{1,0:T(8,128)(2,1)} %param.39) | copy-start | bytes 393220
  134.8 13.2 %copy-start.14 = (f32[4,128,16]{1,2,0:T(8,128)S(1)}, f32[4,128,16]{1,2,0:T(8,128)}, u32[]{:S(2)}) copy-start(f32[4,128,16]{1,2,0:T(8,128)} %param.52) | copy-start | bytes 98308
  134.8 13.3 %copy-start.19 = (f32[4,512]{1,0:T(4,128)S(1)}, f32[4,512]{1,0:T(4,128)}, u32[]{:S(2)}) copy-start(f32[4,512]{1,0:T(4,128)} %param.43) | copy-start | bytes 24580
  134.8 13.3 %copy-start.18 = (f32[4,512]{1,0:T(4,128)S(1)}, f32[4,512]{1,0:T(4,128)}, u32[]{:S(2)}) copy-start(f32[4,512]{1,0:T(4,128)} %param.42) | copy-start | bytes 24580
  134.8 13.3 %copy-start.3 = (bf16[4,128,512]{2,1,0:T(8,128)(2,1)S(1)}, bf16[4,128,512]{2,1,0:T(8,128)(2,1)}, u32[]{:S(2)}) copy-start(bf16[4,128,512]{2,1,0:T(8,128)(2,1)} %param.49) | copy-start | bytes 1572868
  134.8 126.3 %all-reduce.15.cloned.1.call-start = ((), (), s32[]{:S(2)}) async-start(), calls=%async_computation.7 | async-start | bytes 1572864
  135.0 13.1 %copy-start.24 = (pred[4,128]{1,0:T(4,128)(4,1)}, pred[4,128]{1,0:T(4,128)(4,1)S(1)}, u32[]{:S(2)}) copy-start(pred[4,128]{1,0:T(4,128)(4,1)S(1)} %iota_compare_fusion) | copy-start | bytes 1540
  144.5 4.4 copy-start.28
  144.5 5.6 %copy-start.27 = (f32[16]{0:T(128)S(1)}, f32[16]{0:T(128)}, u32[]{:S(2)}) copy-start(f32[16]{0:T(128)} %param.47) | copy-start | bytes 196
  144.5 5.6 %copy-start.12 = (f32[4,128,16]{1,2,0:T(8,128)S(1)}, f32[4,128,16]{1,2,0:T(8,128)}, u32[]{:S(2)}) copy-start(f32[4,128,16]{1,2,0:T(8,128)} %param.51) | copy-start | bytes 98308
  148.0 174.1 %reduce-scatter.6.cloned.1.call-start = ((), (), s32[]{:S(2)}) async-start(), calls=%async_computation.4 | async-start | bytes 24576 | tf_op jit(solution)/shard_map/reduce_scatter | solution.py:29
  148.1 4.4 copy-start.15
  148.1 4.4 copy-start.23
  148.1 4.5 copy-start.16
  148.2 4.5 copy-start.20
  148.2 4.5 copy-start.21
  148.2 4.7 %copy-start.22 = (bf16[128,32]{0,1:T(8,128)(2,1)S(1)}, bf16[128,32]{0,1:T(8,128)(2,1)}, u32[]{:S(2)}) copy-start(bf16[128,32]{0,1:T(8,128)(2,1)} %param.40) | copy-start | bytes 24580
  148.6 114.8 %copy-start.25 = (pred[4,128]{1,0:T(4,128)(4,1)S(1)}, pred[4,128]{1,0:T(4,128)(4,1)}, u32[]{:S(2)}) copy-start(pred[4,128]{1,0:T(4,128)(4,1)} %copy-done.24) | copy-start | bytes 1540
  265.9 5.3 %copy-start.8 = (f32[4,16,64]{2,1,0:T(8,128)S(1)}, f32[4,16,64]{2,1,0:T(8,128)}, u32[]{:S(2)}) copy-start(f32[4,16,64]{2,1,0:T(8,128)} %reshape.84) | copy-start | bytes 49156
  265.9 5.3 %copy-start.9 = (f32[4,16,64]{2,1,0:T(8,128)S(1)}, f32[4,16,64]{2,1,0:T(8,128)}, u32[]{:S(2)}) copy-start(f32[4,16,64]{2,1,0:T(8,128)} %reshape.85) | copy-start | bytes 49156
  265.9 59.3 %copy-start.1 = (bf16[128,2816]{1,0:T(8,128)(2,1)S(1)}, bf16[128,2816]{1,0:T(8,128)(2,1)}, u32[]{:S(2)}) copy-start(bf16[128,2816]{1,0:T(8,128)(2,1)} %param.57) | copy-start | bytes 2162692
  267.8 59.1 %copy-start.2 = (bf16[128,2816]{1,0:T(8,128)(2,1)S(1)}, bf16[128,2816]{1,0:T(8,128)(2,1)}, u32[]{:S(2)}) copy-start(bf16[128,2816]{1,0:T(8,128)(2,1)} %param.58) | copy-start | bytes 2162692
  318.6 127.6 %all-reduce.13.cloned.1.call-start = ((), (), s32[]{:S(2)}) async-start(), calls=%async_computation.6 | async-start | bytes 2883584 | tf_op jit(solution)/shard_map/psum | solution.py:45
  322.8 0.6 copy-start.10
  328.8 127.1 %reduce-scatter.8.cloned.1.call-start = ((), (), s32[]{:S(2)}) async-start(), calls=%async_computation.5 | async-start | bytes 24576 | tf_op jit(solution)/shard_map/reduce_scatter | solution.py:29
  328.9 3.6 collective-permute-start.4
  332.6 3.6 collective-permute-start.5
  336.1 3.8 collective-permute-start.6
  340.0 4.5 collective-permute-start.7
  446.2 9.7 %copy-start.11 = (bf16[32,128]{1,0:T(8,128)(2,1)S(1)}, bf16[32,128]{1,0:T(8,128)(2,1)}, u32[]{:S(2)}) copy-start(bf16[32,128]{1,0:T(8,128)(2,1)} %copy-done.10) | copy-start | bytes 24580
Sparse Core Ops, SparseCore 0:
  13.5 118.6 all-reduce.16
  135.0 6.9 reduce-scatter.3
  148.1 113.0 all-reduce.14
  318.7 3.3 reduce-scatter.5
  328.9 117.2 all-reduce.12
  448.9 6.9 reduce-scatter.7
